TPU v7x, 32 devices: a whole 2x2x4 slice. The times are simulated.
32 devices in a mesh: ep: 8 (over z, x), tp: 4 (over y, core).
Axes of the slice: x: 2, y: 2, z: 4, core: 2. Of those that a mesh axis runs over, the one named last changes fastest.
Arguments:
- tokens: bfloat16 [384, 1024], P('ep'), may hold values from -6 to 6
- head_state: float32 [384, 8, 64, 64], P('ep', 'tp'), may hold values from -6 to 6
- recept_weight: bfloat16 [1024, 512], P(None, 'tp'), may hold values from -0.1875 to 0.1875
- key_weight: bfloat16 [1024, 512], P(None, 'tp'), may hold values from -0.1875 to 0.1875
- value_weight: bfloat16 [1024, 512], P(None, 'tp'), may hold values from -0.1875 to 0.1875
- decay_down_factor: bfloat16 [1024, 64], replicated, may hold values from -0.1875 to 0.1875
- decay_up_factor: bfloat16 [64, 512], P(None, 'tp'), may hold values from -0.75 to 0.75
- decay_base: float32 [512], P('tp'), may hold values from -5 to 3
- rate_down_factor: bfloat16 [1024, 64], replicated, may hold values from -0.1875 to 0.1875
- rate_up_factor: bfloat16 [64, 512], P(None, 'tp'), may hold values from -0.75 to 0.75
- rate_base: float32 [512], P('tp'), may hold values from -3 to 3
- head_gain: float32 [512], P('tp'), may hold values from 0.1 to 1.9
- out_weight: bfloat16 [512, 1024], P('tp'), may hold values from -0.25 to 0.25
- route_experts: int32 [384, 4], P('ep'), may hold values from 0 to 7, all different within a row; in each aligned block of 48 rows (0 to 47, 48 to 95, ...) at most 48 rows name the same one
- route_weights: float32 [384, 4], P('ep'), may hold values from 0.03 to 0.2
- expert_gate: bfloat16 [8, 1024, 1024], P('ep', None, 'tp'), may hold values from -1 to 1
- expert_up: bfloat16 [8, 1024, 1024], P('ep', None, 'tp'), may hold values from -1 to 1
- expert_down: bfloat16 [8, 1024, 1024], P('ep', 'tp'), may hold values from -0.1875 to 0.1875
Outputs:
- layer_out: bfloat16 [384, 1024], P('ep', 'tp')
- new_state: float32 [384, 8, 64, 64], P('ep', 'tp')
Inputs may be any that keep to these rules, and one draw needn't show every extreme that they name: `route_experts`: each row names 4 different experts. In each aligned block of 48 rows no expert is named by more than 48 rows, a bound that some block reaches.
All inputs are finite; a program needn't handle non-finite values.
Results may differ from a plain program's by a relative error of at most 0.02.
Values may be sent and summed in bfloat16 or wider, within the bound.
No kernel may reach another device: no remote copies, remote signals or barrier semaphores. Data moves between devices by JAX's collectives and lax.ppermute only.
A program may use at most 128 MiB of HBM per device.

v0:
```python
import jax
import jax.numpy as jnp
from jax import lax
from jax.sharding import PartitionSpec as P

NORM_EPS = 1e-05
GROUP_EPS = 0.00064
UNIT_EPS = 1e-06
CLAMP_LIMIT = 7.0
GLU_ALPHA = 1.702


def row_norm(values):
    return values * lax.rsqrt(jnp.mean(values * values, axis=-1, keepdims=True) + NORM_EPS)


def clamped_unit(gate_pre, up_pre):
    gated = jnp.minimum(gate_pre, CLAMP_LIMIT)
    linear = jnp.clip(up_pre, -CLAMP_LIMIT, CLAMP_LIMIT)
    return gated * jax.nn.sigmoid(GLU_ALPHA * gated) * (linear + 1.0)


def update_heads(head_state, recept, keys, values, decay_rate, rate_gate, head_gain):
    seq_count, head_count, head_size = head_state.shape[:3]

    def by_heads(operand):
        return operand.astype(jnp.float32).reshape(seq_count, head_count, head_size)

    recept_heads = by_heads(recept)
    key_heads = by_heads(keys)
    value_heads = by_heads(values)
    decay_heads = by_heads(decay_rate)
    rate_heads = by_heads(rate_gate)
    unit_key = key_heads * lax.rsqrt(
        jnp.sum(key_heads * key_heads, axis=-1, keepdims=True) + UNIT_EPS
    )
    highest = lax.Precision.HIGHEST
    state_unit = jnp.einsum("shvk,shk->shv", head_state, unit_key, precision=highest)
    new_state = (
        head_state * decay_heads[:, :, None, :]
        - state_unit[..., None] * (unit_key * rate_heads)[:, :, None, :]
        + value_heads[..., None] * (key_heads * rate_heads)[:, :, None, :]
    )
    head_out = jnp.einsum("shvk,shk->shv", new_state, recept_heads, precision=highest)
    centre = jnp.mean(head_out, axis=-1, keepdims=True)
    spread = jnp.mean(jnp.square(head_out - centre), axis=-1, keepdims=True)
    normed_heads = (head_out - centre) * lax.rsqrt(spread + GROUP_EPS)
    mixed = (normed_heads.reshape(seq_count, -1) * head_gain).astype(jnp.bfloat16)
    return (new_state, mixed)


def local(
    tokens,
    head_state,
    recept_weight,
    key_weight,
    value_weight,
    decay_down_factor,
    decay_up_factor,
    decay_base,
    rate_down_factor,
    rate_up_factor,
    rate_base,
    head_gain,
    out_weight,
    route_experts,
    route_weights,
    expert_gate,
    expert_up,
    expert_down,
):
    tokens_float = tokens.astype(jnp.float32)
    normed = row_norm(tokens_float).astype(jnp.bfloat16)
    recept = jnp.dot(normed, recept_weight, preferred_element_type=jnp.float32).astype(jnp.bfloat16)
    keys = jnp.dot(normed, key_weight, preferred_element_type=jnp.float32).astype(jnp.bfloat16)
    values = jnp.dot(normed, value_weight, preferred_element_type=jnp.float32).astype(jnp.bfloat16)
    decay_low = jnp.tanh(
        jnp.dot(normed, decay_down_factor, preferred_element_type=jnp.float32)
    ).astype(jnp.bfloat16)
    rate_low = jnp.dot(normed, rate_down_factor, preferred_element_type=jnp.float32).astype(
        jnp.bfloat16
    )
    decay_pre = decay_base + jnp.dot(decay_low, decay_up_factor, preferred_element_type=jnp.float32)
    decay_rate = jnp.exp(-jnp.exp(-jax.nn.softplus(-decay_pre) - 0.5))
    rate_gate = jax.nn.sigmoid(
        rate_base + jnp.dot(rate_low, rate_up_factor, preferred_element_type=jnp.float32)
    )
    new_state, mixed = update_heads(
        head_state, recept, keys, values, decay_rate, rate_gate, head_gain
    )
    partial_value = jnp.dot(mixed, out_weight, preferred_element_type=jnp.float32).astype(
        jnp.bfloat16
    )
    partial_value = lax.optimization_barrier(partial_value).astype(jnp.float32)
    summed = lax.psum(partial_value.astype(jnp.bfloat16), "tp").astype(jnp.float32)
    residual = (tokens_float + summed).astype(jnp.bfloat16)
    expert_input = row_norm(residual.astype(jnp.float32)).astype(jnp.bfloat16)
    seq_count, top_count = route_experts.shape
    expert_count = lax.axis_size("ep")
    capacity = max(2, (2 * seq_count * top_count + expert_count - 1) // expert_count)
    column_count = expert_input.shape[1] // lax.axis_size("tp")
    column_start = lax.axis_index("tp") * column_count
    flat_routes = route_experts.reshape(-1)
    onehot = (flat_routes[:, None] == jnp.arange(expert_count, dtype=jnp.int32)[None, :]).astype(
        jnp.int32
    )
    earlier = jnp.cumsum(onehot, axis=0) - onehot
    target = flat_routes * capacity + jnp.sum(earlier * onehot, axis=1)
    slot_ids = jnp.arange(expert_count * capacity, dtype=jnp.int32)
    dispatch_map = jnp.any(
        slot_ids[:, None, None] == target.reshape(seq_count, top_count)[None], axis=-1
    )
    dispatch_map = dispatch_map.astype(jnp.bfloat16)
    outgoing = lax.dynamic_slice_in_dim(expert_input, column_start, column_count, 1)
    buffer = jnp.dot(dispatch_map, outgoing, preferred_element_type=jnp.float32).astype(
        jnp.bfloat16
    )
    buffer = buffer.reshape(expert_count, capacity, outgoing.shape[1])
    slot_rows = lax.all_gather(
        lax.all_to_all(buffer, "ep", split_axis=0, concat_axis=0, tiled=True),
        "tp",
        axis=2,
        tiled=True,
    )
    source_count, slot_count, model_width = slot_rows.shape
    flat_rows = slot_rows.reshape(-1, model_width)
    gate_pre = jnp.dot(flat_rows, expert_gate[0], preferred_element_type=jnp.float32)
    up_pre = jnp.dot(flat_rows, expert_up[0], preferred_element_type=jnp.float32)
    activated = clamped_unit(gate_pre, up_pre).astype(jnp.bfloat16)
    part_out = jnp.dot(activated, expert_down[0], preferred_element_type=jnp.float32).astype(
        jnp.bfloat16
    )
    part_out = lax.optimization_barrier(part_out).astype(jnp.float32)
    part_out = part_out.reshape(source_count, slot_count, model_width)
    shares = lax.psum_scatter(part_out.astype(jnp.bfloat16), "tp", scatter_dimension=2, tiled=True)
    returned = lax.all_to_all(shares, "ep", split_axis=0, concat_axis=0, tiled=True)
    picked = returned.reshape(expert_count * capacity, column_count)[target]
    picked = picked.reshape(seq_count, top_count, column_count).astype(jnp.float32)
    mixture = jnp.sum(route_weights[:, :, None] * picked, axis=1)
    own_residual = lax.dynamic_slice_in_dim(residual, column_start, column_count, 1).astype(
        jnp.float32
    )
    layer_out = (own_residual + mixture).astype(jnp.bfloat16)
    return (layer_out, new_state)


def solution(mesh):
    in_specs = (
        P("ep", None),
        P("ep", "tp", None, None),
        P(None, "tp"),
        P(None, "tp"),
        P(None, "tp"),
        P(),
        P(None, "tp"),
        P("tp"),
        P(),
        P(None, "tp"),
        P("tp"),
        P("tp"),
        P("tp", None),
        P("ep", None),
        P("ep", None),
        P("ep", None, "tp"),
        P("ep", None, "tp"),
        P("ep", "tp", None),
    )
    out_specs = (P("ep", "tp"), P("ep", "tp", None, None))
    return jax.shard_map(local, mesh=mesh, in_specs=in_specs, out_specs=out_specs, check_vma=False)
```

profile of v0, /device:TPU:0, one launch (start us, length us, event | category | flops | bytes accessed | tf_op | source)
XLA Modules:
  0.0 132.7 jit_solution(9616172341950078391)
XLA Ops:
  7.2 0.0 all-reduce.3.cloned.1.call-start
  7.2 1.1 fusion.22
  8.3 1.2 fusion.10
  9.5 0.1 reshape.151
  9.6 0.1 multiply_reduce_fusion.3
  9.8 1.3 %fusion.6 = f32[48,128]{1,0:T(8,128)S(1)} fusion(bf16[64,128]{1,0:T(8,128)(2,1)} %param.27, bf16[1024,64]{0,1:T(8,128)(2,1)} %param.26, f32[128]{0:T(128)} %param.28, bf16[48,1024]{1,0:T(8,128)(2,1)} %param.18, f32[48]{0:T(128)S(1)} %add_rsqrt_fusion.3), kind=kOutput, calls=%fused_computation.14 | convolution fusion | flops 7252992 | bytes 271040 | tf_op jit(solution)/shard_map/dot_general | solution.py:86
  11.1 0.1 reshape.142
  11.2 1.4 %fusion.35 = f32[48,128]{1,0:T(8,128)S(1)} fusion(bf16[64,128]{1,0:T(8,128)(2,1)} %param.24, bf16[1024,64]{0,1:T(8,128)(2,1)} %param.23, f32[128]{0:T(128)} %param.25, bf16[48,1024]{1,0:T(8,128)(2,1)} %param.18, f32[48]{0:T(128)S(1)} %add_rsqrt_fusion.3), kind=kOutput, calls=%fused_computation.59 | convolution fusion | flops 7296000 | bytes 271040 | tf_op jit(solution)/shard_map/dot_general | solution.py:83
  12.6 0.1 mul.155
  12.7 1.2 fusion.9
  13.9 0.1 reshape.152
  14.0 1.2 convolution_convert_fusion.3
  15.2 0.1 reshape.168
  15.3 0.1 fusion.54
  15.5 7.0 %fusion.55 = f32[48,2,1,64]{3,2,1,0:T(1,128)S(1)} fusion(f32[48,2,64,1]{2,3,1,0:T(1,128)S(1)} %bitcast.53, f32[48,2,64,64]{3,2,1,0:T(8,128)} %param.19), kind=kOutput, calls=%fused_computation.87 | convolution fusion | flops 4718592 | bytes 1622016 | tf_op jit(solution)/shard_map/shvk,shk->shv/dot_general | solution.py:38
  22.5 2.1 %multiply_add_fusion = f32[48,2,64,64]{3,2,1,0:T(8,128)S(1)} fusion(f32[48,2,64,64]{3,2,1,0:T(8,128)S(1)} %copy-done.1, f32[48,2,64]{2,1,0:T(2,128)S(1)} %get-tuple-element.6, f32[48,2,64]{2,1,0:T(2,128)S(1)} %reshape.152, f32[48,2,64]{2,1,0:T(2,128)S(1)} %get-tuple-element.4, f32[48,2,64]{2,1,0:T(2,128)S(1)} %bitcast.52, f32[48,2,64]{2,1,0:T(2,128)S(1)} %mul.155), kind=kLoop, calls=%fused_computation.1 | loop fusion | flops 1966080 | bytes 3268608 | tf_op jit(solution)/shard_map/add | solution.py:40
  24.6 1.7 %copy-done.2 = f32[48,2,64,64]{3,2,1,0:T(8,128)} copy-done((f32[48,2,64,64]{3,2,1,0:T(8,128)}, f32[48,2,64,64]{3,2,1,0:T(8,128)S(1)}, u32[]{:S(2)}) %copy-start.2) | copy-done | bytes 1572888
  26.2 2.5 %fusion.56 = f32[48,2,1,64]{3,2,1,0:T(1,128)S(1)} fusion(f32[48,2,64,64]{3,2,1,0:T(8,128)S(1)} %multiply_add_fusion, bf16[48,2,64,1]{2,3,1,0:T(2,128)(2,1)S(1)} %reshape.168), kind=kOutput, calls=%fused_computation.88 | convolution fusion | flops 4718592 | bytes 1609728 | tf_op jit(solution)/shard_map/shvk,shk->shv/dot_general | solution.py:44
  28.8 0.1 reduce_sum.69
  28.9 0.2 multiply_reduce_fusion.2
  29.2 0.2 subtract_multiply_fusion
  29.3 0.1 reshape.144
  29.4 0.8 convolution_convert_fusion.2
  30.2 0.0 all-reduce.3.cloned.1.call-update
  30.3 0.0 reduce-scatter.2.cloned.1.call-start
  30.3 0.1 copy.34
  30.4 0.1 eq.36
  30.6 0.6 reduce-window.6
  31.1 0.2 slice_reduce_fusion
  31.4 0.1 add_bitcast_fusion
  31.5 0.1 reduce_sum.72
  31.6 0.1 copy.36
  31.7 0.1 fusion.21
  31.8 33.0 %all-reduce.3.cloned.1.call-done = bf16[48,1024]{1,0:T(8,128)(2,1)} async-done(((bf16[48,1024]{1,0:T(8,128)(2,1)}), bf16[48,1024]{1,0:T(8,128)(2,1)}) %all-reduce.3.cloned.1.call-update) | async-done | bytes 98320 | tf_op jit(solution)/shard_map/psum | solution.py:95
  64.8 1.0 multiply_reduce_fusion.1
  65.9 0.3 convolution_convert_fusion.1
  66.2 13.1 %all_to_all.10 = bf16[8,48,256]{2,1,0:T(8,128)(2,1)S(1)} all-to-all(bf16[8,48,256]{2,1,0:T(8,128)(2,1)S(1)} %bitcast.48), channel_id=1, replica_groups=mesh['ep'=8,'tp'=4] {'ep'}, dimensions={0} | all-to-all | bytes 393216 | tf_op jit(solution)/shard_map/all_to_all | solution.py:120
  79.3 7.6 %all_gather.3 = bf16[8,48,1024]{2,1,0:T(8,128)(2,1)S(1)} all-gather(bf16[8,48,256]{2,1,0:T(8,128)(2,1)S(1)} %all_to_all.10), channel_id=1, replica_groups=mesh['ep'=8,'tp'=4] {'tp'}, dimensions={2}, use_global_device_ids=true | all-gather | bytes 983040 | tf_op jit(solution)/shard_map/all_gather | solution.py:119
  86.9 0.4 convolution_minimum_fusion
  87.3 1.9 %convolution_convert_fusion = bf16[384,1024]{1,0:T(8,128)(2,1)} fusion(bf16[384,1024]{1,0:T(8,128)(2,1)S(1)} %bitcast.46, bf16[1,256,1024]{2,1,0:T(8,128)(2,1)S(1)} %copy-done, bf16[1,1024,256]{2,1,0:T(8,128)(2,1)S(1)} %copy-done.9, f32[384,256]{1,0:T(8,128)S(1)} %convolution_minimum_fusion), kind=kOutput, calls=%fused_computation.2 | convolution fusion | flops 403931136 | bytes 3014656 | tf_op jit(solution)/shard_map/dot_general | solution.py:130
  89.2 21.5 %reduce-scatter.2.cloned.1.call-done = bf16[8,48,256]{2,1,0:T(8,128)(2,1)} async-done(((bf16[8,48,1024]{2,1,0:T(8,128)(2,1)}), bf16[8,48,256]{2,1,0:T(8,128)(2,1)}) %reduce-scatter.2.cloned.1.call-update) | async-done | bytes 196624 | tf_op jit(solution)/shard_map/reduce_scatter | solution.py:135
  110.6 5.5 %all-to-all-start.1 = ((bf16[8,48,256]{2,1,0:T(8,128)(2,1)}), bf16[8,48,256]{2,1,0:T(8,128)(2,1)S(1)}, u32[]{:S(2)}, u32[]{:S(2)}) async-start(bf16[8,48,256]{2,1,0:T(8,128)(2,1)} %reduce-scatter.2.cloned.1.call-done), calls=%async_computation.2 | async-start | bytes 393216 | tf_op jit(solution)/shard_map/all_to_all | solution.py:136
  116.2 0.1 mul.187
  116.3 0.1 copy.33
  116.4 7.6 %all-to-all-done.1 = bf16[8,48,256]{2,1,0:T(8,128)(2,1)S(1)} async-done(((bf16[8,48,256]{2,1,0:T(8,128)(2,1)}), bf16[8,48,256]{2,1,0:T(8,128)(2,1)S(1)}, u32[]{:S(2)}, u32[]{:S(2)}) %all-to-all-start.1) | async-done | bytes 196640 | tf_op jit(solution)/shard_map/all_to_all | solution.py:136
  123.9 1.0 gather_fusion
  125.0 0.2 multiply_reduce_fusion
  125.2 0.6 add_convert_fusion
  (35 shorter events, 0.3 us)
Async XLA Ops:
  7.2 80.1 %copy-start = (bf16[1,256,1024]{2,1,0:T(8,128)(2,1)S(1)}, bf16[1,256,1024]{2,1,0:T(8,128)(2,1)}, u32[]{:S(2)}) copy-start(bf16[1,256,1024]{2,1,0:T(8,128)(2,1)} %param.35) | copy-start | bytes 1572868
  7.2 57.6 %all-reduce.3.cloned.1.call-start = ((), (), s32[]{:S(2)}) async-start(), calls=%async_computation.3 | async-start | bytes 196608 | tf_op jit(solution)/shard_map/psum | solution.py:95
  15.3 7.2 %copy-start.1 = (f32[48,2,64,64]{3,2,1,0:T(8,128)S(1)}, f32[48,2,64,64]{3,2,1,0:T(8,128)}, u32[]{:S(2)}) copy-start(f32[48,2,64,64]{3,2,1,0:T(8,128)} %param.19) | copy-start | bytes 4718596
  24.6 1.7 %copy-start.2 = (f32[48,2,64,64]{3,2,1,0:T(8,128)}, f32[48,2,64,64]{3,2,1,0:T(8,128)S(1)}, u32[]{:S(2)}) copy-start(f32[48,2,64,64]{3,2,1,0:T(8,128)S(1)} %multiply_add_fusion) | copy-start | bytes 4718596
  26.2 3.2 %copy-start.5 = (bf16[128,1024]{1,0:T(8,128)(2,1)S(1)}, bf16[128,1024]{1,0:T(8,128)(2,1)}, u32[]{:S(2)}) copy-start(bf16[128,1024]{1,0:T(8,128)(2,1)} %param.30) | copy-start | bytes 786436
  26.2 3.2 %copy-start.8 = (f32[128]{0:T(128)S(1)}, f32[128]{0:T(128)}, u32[]{:S(2)}) copy-start(f32[128]{0:T(128)} %param.29) | copy-start | bytes 1540
  26.2 4.1 %copy-start.6 = (s32[48,4]{0,1:T(4,128)S(1)}, s32[48,4]{0,1:T(4,128)}, u32[]{:S(2)}) copy-start(s32[48,4]{0,1:T(4,128)} %param.31) | copy-start | bytes 2308
  26.2 38.6 %copy-start.3 = (bf16[48,1024]{1,0:T(8,128)(2,1)S(1)}, bf16[48,1024]{1,0:T(8,128)(2,1)}, u32[]{:S(2)}) copy-start(bf16[48,1024]{1,0:T(8,128)(2,1)} %param.18) | copy-start | bytes 294916
  26.2 60.6 %copy-start.4 = (bf16[1,1024,256]{2,1,0:T(8,128)(2,1)S(1)}, bf16[1,1024,256]{2,1,0:T(8,128)(2,1)}, u32[]{:S(2)}) copy-start(bf16[1,1024,256]{2,1,0:T(8,128)(2,1)} %param.33) | copy-start | bytes 1572868
  28.8 58.5 %copy-start.9 = (bf16[1,1024,256]{2,1,0:T(8,128)(2,1)S(1)}, bf16[1,1024,256]{2,1,0:T(8,128)(2,1)}, u32[]{:S(2)}) copy-start(bf16[1,1024,256]{2,1,0:T(8,128)(2,1)} %param.34) | copy-start | bytes 1572868
  30.3 80.4 %reduce-scatter.2.cloned.1.call-start = ((), (), s32[]{:S(2)}) async-start(), calls=%async_computation.4 | async-start | bytes 983040 | tf_op jit(solution)/shard_map/reduce_scatter | solution.py:135
  87.3 29.0 %copy-start.7 = (f32[48,4]{0,1:T(4,128)S(1)}, f32[48,4]{0,1:T(4,128)}, u32[]{:S(2)}) copy-start(f32[48,4]{0,1:T(4,128)} %param.32) | copy-start | bytes 2308
  110.6 13.3 %all-to-all-start.1 = ((bf16[8,48,256]{2,1,0:T(8,128)(2,1)}), bf16[8,48,256]{2,1,0:T(8,128)(2,1)S(1)}, u32[]{:S(2)}, u32[]{:S(2)}) async-start(bf16[8,48,256]{2,1,0:T(8,128)(2,1)} %reduce-scatter.2.cloned.1.call-done), calls=%async_computation.2 | async-start | bytes 393216 | tf_op jit(solution)/shard_map/all_to_all | solution.py:136
Sparse Core Ops, SparseCore 0:
  30.4 34.3 all-reduce.2
  89.3 21.2 reduce-scatter.1
where the time goes:
time: 133 us
  waiting for transfers between devices  62 us (47%)
  blocking collectives  20.7 us (16%)
  matrix products  19.3 us (15%)
  between operations  14.4 us (11%)
  other arithmetic  6.64 us (5%)
  starting transfers between devices  5.59 us (4%)
  local copies, waits for them, and re-layouts  4.08 us (3%)
    psum x1, waiting for transfers between devices, local(): lax.psum(partial_value.astype(jnp.bfloat16), 'tp').astype(jnp.float32)  33 us
    reduce_scatter x1, waiting for transfers between devices, local(): lax.psum_scatter(part_out.astype(jnp.bfloat16), 'tp', scatter_dimension=2...  21.5 us
    all_to_all x1, blocking collectives, local(): lax.all_to_all(buffer, 'ep', split_axis=0, concat_axis=0, tiled=True)  13.1 us
    all_gather x1, blocking collectives, local(): lax.all_gather(lax.all_to_all(buffer, 'ep', split_axis=0, concat_axis=0,...  7.58 us
    all_to_all x1, waiting for transfers between devices, local(): lax.all_to_all(shares, 'ep', split_axis=0, concat_axis=0, tiled=True)  7.57 us
    dot_general x1, matrix products, update_heads(): jnp.einsum('shvk,shk->shv', head_state, unit_key, precision=highest)  7.01 us
    all_to_all x1, starting transfers between devices, local(): lax.all_to_all(shares, 'ep', split_axis=0, concat_axis=0, tiled=True)  5.51 us
  transfers between devices with their start and end apart: 3, of which 3 were waited for; matrix products, arithmetic and copies ran while one was open for 1% of the time, Pallas kernels for 0%

commit v1 on v0

--- a/solution.py
+++ b/solution.py
@@ -8,6 +8,10 @@
 UNIT_EPS = 1e-06
 CLAMP_LIMIT = 7.0
 GLU_ALPHA = 1.702
+
+
+def _fix_cube(vals, a_name):
+    return lax.all_gather(vals, axis_name=a_name).sum(axis=0)
 
 
 def row_norm(values):
@@ -92,7 +96,7 @@
         jnp.bfloat16
     )
     partial_value = lax.optimization_barrier(partial_value).astype(jnp.float32)
-    summed = lax.psum(partial_value.astype(jnp.bfloat16), "tp").astype(jnp.float32)
+    summed = _fix_cube(partial_value.astype(jnp.bfloat16), a_name="tp").astype(jnp.float32)
     residual = (tokens_float + summed).astype(jnp.bfloat16)
     expert_input = row_norm(residual.astype(jnp.float32)).astype(jnp.bfloat16)
     seq_count, top_count = route_experts.shape

time: 133 us -> 108 us (0.81)
  waiting for transfers between devices: 62 us -> 28.9 us
  blocking collectives: 20.7 us -> 30.3 us
    psum x1 -> x0, waiting for transfers between devices: 33 us -> none  [local(): lax.psum(partial_value.astype(jnp.bfloat16), 'tp').astype(jnp.float32)]
    all_gather x0 -> x1, blocking collectives: none -> 7.96 us  [_fix_cube(): return lax.all_gather(vals, axis_name=a_name).sum(axis=0)]
  transfers between devices with their start and end apart: 3 -> 2, of which waited for: 3 -> 2; matrix products, arithmetic and copies ran while one was open for 1% -> 0% of each run, Pallas kernels for 0% -> 0%
where the time goes in v1:
time: 108 us
  blocking collectives  30.3 us (28%)
  waiting for transfers between devices  28.9 us (27%)
  matrix products  18.6 us (17%)
  between operations  14.4 us (13%)
  other arithmetic  5.8 us (5%)
  starting transfers between devices  5.57 us (5%)
  local copies, waits for them, and re-layouts  4.08 us (4%)
    reduce_scatter x1, waiting for transfers between devices, local(): lax.psum_scatter(part_out.astype(jnp.bfloat16), 'tp', scatter_dimension=2...  21.3 us
    all_to_all x1, blocking collectives, local(): lax.all_to_all(buffer, 'ep', split_axis=0, concat_axis=0, tiled=True)  14.1 us
    all_gather x1, blocking collectives, local(): lax.all_gather(lax.all_to_all(buffer, 'ep', split_axis=0, concat_axis=0,...  8.26 us
    all_gather x1, blocking collectives, _fix_cube(): return lax.all_gather(vals, axis_name=a_name).sum(axis=0)  7.96 us
    all_to_all x1, waiting for transfers between devices, local(): lax.all_to_all(shares, 'ep', split_axis=0, concat_axis=0, tiled=True)  7.56 us
    dot_general x1, matrix products, update_heads(): jnp.einsum('shvk,shk->shv', head_state, unit_key, precision=highest)  7.01 us
    all_to_all x1, starting transfers between devices, local(): lax.all_to_all(shares, 'ep', split_axis=0, concat_axis=0, tiled=True)  5.53 us
    dot_general x1, matrix products, update_heads(): jnp.einsum('shvk,shk->shv', new_state, recept_heads, precision=highest)  2.55 us
  transfers between devices with their start and end apart: 2, of which 2 were waited for; matrix products, arithmetic and copies ran while one was open for 0% of the time, Pallas kernels for 0%

profile of v1, /device:TPU:0, one launch (start us, length us, event | category | flops | bytes accessed | tf_op | source)
XLA Modules:
  0.0 107.6 jit_solution(3199308004516936415)
XLA Ops:
  7.2 0.0 reduce-scatter.2.cloned.1.call-start
  7.2 1.1 fusion.22
  8.3 1.2 %fusion.10 = f32[48,128]{1,0:T(8,128)S(1)} fusion(bf16[1024,128]{1,0:T(8,128)(2,1)} %param.21, bf16[48,1024]{1,0:T(8,128)(2,1)} %param.18, f32[48]{0:T(128)S(1)} %add_rsqrt_fusion.3), kind=kOutput, calls=%fused_computation.24 | convolution fusion | flops 12742656 | bytes 385216 | tf_op jit(solution)/shard_map/dot_general | solution.py:79
  9.5 0.1 reshape.151
  9.6 0.1 multiply_reduce_fusion.3
  9.8 1.3 %fusion.6 = f32[48,128]{1,0:T(8,128)S(1)} fusion(bf16[64,128]{1,0:T(8,128)(2,1)} %param.27, bf16[1024,64]{0,1:T(8,128)(2,1)} %param.26, f32[128]{0:T(128)} %param.28, bf16[48,1024]{1,0:T(8,128)(2,1)} %param.18, f32[48]{0:T(128)S(1)} %add_rsqrt_fusion.3), kind=kOutput, calls=%fused_computation.14 | convolution fusion | flops 7252992 | bytes 271040 | tf_op jit(solution)/shard_map/dot_general | solution.py:90
  11.1 0.1 reshape.142
  11.2 1.4 %fusion.35 = f32[48,128]{1,0:T(8,128)S(1)} fusion(bf16[64,128]{1,0:T(8,128)(2,1)} %param.24, bf16[1024,64]{0,1:T(8,128)(2,1)} %param.23, f32[128]{0:T(128)} %param.25, bf16[48,1024]{1,0:T(8,128)(2,1)} %param.18, f32[48]{0:T(128)S(1)} %add_rsqrt_fusion.3), kind=kOutput, calls=%fused_computation.59 | convolution fusion | flops 7296000 | bytes 271040 | tf_op jit(solution)/shard_map/dot_general | solution.py:87
  12.6 0.1 mul.155
  12.7 1.2 %fusion.9 = f32[48,128]{1,0:T(8,128)S(1)} fusion(bf16[1024,128]{1,0:T(8,128)(2,1)} %param.22, bf16[48,1024]{1,0:T(8,128)(2,1)} %param.18, f32[48]{0:T(128)S(1)} %add_rsqrt_fusion.3), kind=kOutput, calls=%fused_computation.21 | convolution fusion | flops 12742656 | bytes 385216 | tf_op jit(solution)/shard_map/dot_general | solution.py:80
  13.9 0.1 reshape.152
  14.0 1.2 %convolution_convert_fusion.3 = bf16[48,128]{1,0:T(8,128)(2,1)S(1)} fusion(bf16[1024,128]{1,0:T(8,128)(2,1)} %param.20, bf16[48,1024]{1,0:T(8,128)(2,1)} %param.18, f32[48]{0:T(128)S(1)} %add_rsqrt_fusion.3), kind=kOutput, calls=%fused_computation.19 | convolution fusion | flops 12736512 | bytes 372928 | tf_op jit(solution)/shard_map/dot_general | solution.py:78
  15.3 0.1 reshape.169
  15.4 0.1 fusion.54
  15.5 7.0 %fusion.55 = f32[48,2,1,64]{3,2,1,0:T(1,128)S(1)} fusion(f32[48,2,64,1]{2,3,1,0:T(1,128)S(1)} %bitcast.55, f32[48,2,64,64]{3,2,1,0:T(8,128)} %param.19), kind=kOutput, calls=%fused_computation.87 | convolution fusion | flops 4718592 | bytes 1622016 | tf_op jit(solution)/shard_map/shvk,shk->shv/dot_general | solution.py:42
  22.5 2.1 %multiply_add_fusion = f32[48,2,64,64]{3,2,1,0:T(8,128)S(1)} fusion(f32[48,2,64,64]{3,2,1,0:T(8,128)S(1)} %copy-done.1, f32[48,2,64]{2,1,0:T(2,128)S(1)} %get-tuple-element.6, f32[48,2,64]{2,1,0:T(2,128)S(1)} %reshape.152, f32[48,2,64]{2,1,0:T(2,128)S(1)} %get-tuple-element.4, f32[48,2,64]{2,1,0:T(2,128)S(1)} %bitcast.54, f32[48,2,64]{2,1,0:T(2,128)S(1)} %mul.155), kind=kLoop, calls=%fused_computation.1 | loop fusion | flops 1966080 | bytes 3268608 | tf_op jit(solution)/shard_map/add | solution.py:44
  24.6 1.7 %copy-done.2 = f32[48,2,64,64]{3,2,1,0:T(8,128)} copy-done((f32[48,2,64,64]{3,2,1,0:T(8,128)}, f32[48,2,64,64]{3,2,1,0:T(8,128)S(1)}, u32[]{:S(2)}) %copy-start.2) | copy-done | bytes 1572888
  26.2 2.5 %fusion.56 = f32[48,2,1,64]{3,2,1,0:T(1,128)S(1)} fusion(f32[48,2,64,64]{3,2,1,0:T(8,128)S(1)} %multiply_add_fusion, bf16[48,2,64,1]{2,3,1,0:T(2,128)(2,1)S(1)} %reshape.169), kind=kOutput, calls=%fused_computation.88 | convolution fusion | flops 4718592 | bytes 1609728 | tf_op jit(solution)/shard_map/shvk,shk->shv/dot_general | solution.py:48
  28.8 0.1 reduce_sum.81
  28.9 0.2 multiply_reduce_fusion.2
  29.2 0.2 subtract_multiply_fusion
  29.3 0.1 reshape.144
  29.4 0.2 convolution_convert_fusion.2
  29.6 8.0 %all-gather = bf16[192,1024]{1,0:T(8,128)(2,1)S(1)} all-gather(bf16[48,1024]{1,0:T(8,128)(2,1)S(1)} %convolution_convert_fusion.2), channel_id=2, replica_groups=mesh['ep'=8,'tp'=4] {'tp'}, dimensions={0}, use_global_device_ids=true | all-gather | bytes 491520 | tf_op jit(solution)/shard_map/all_gather | solution.py:14
  37.6 0.1 reduce_sum.83
  37.7 0.1 multiply_reduce_fusion.1
  37.8 0.1 copy.34
  37.9 0.1 eq.36
  38.1 0.6 reduce-window.6
  38.6 0.2 slice_reduce_fusion
  38.9 0.1 add_bitcast_fusion
  39.0 0.1 reduce_sum.85
  39.1 0.1 copy.36
  39.2 0.1 fusion.21
  39.3 0.3 convolution_convert_fusion.1
  39.6 14.1 %all_to_all.10 = bf16[8,48,256]{2,1,0:T(8,128)(2,1)S(1)} all-to-all(bf16[8,48,256]{2,1,0:T(8,128)(2,1)S(1)} %bitcast.50), channel_id=1, replica_groups=mesh['ep'=8,'tp'=4] {'ep'}, dimensions={0} | all-to-all | bytes 393216 | tf_op jit(solution)/shard_map/all_to_all | solution.py:124
  53.7 8.3 %all_gather.11 = bf16[8,48,1024]{2,1,0:T(8,128)(2,1)S(1)} all-gather(bf16[8,48,256]{2,1,0:T(8,128)(2,1)S(1)} %all_to_all.10), channel_id=1, replica_groups=mesh['ep'=8,'tp'=4] {'tp'}, dimensions={2}, use_global_device_ids=true | all-gather | bytes 983040 | tf_op jit(solution)/shard_map/all_gather | solution.py:123
  62.0 0.4 convolution_minimum_fusion
  62.4 1.9 %convolution_convert_fusion = bf16[384,1024]{1,0:T(8,128)(2,1)} fusion(bf16[384,1024]{1,0:T(8,128)(2,1)S(1)} %bitcast.47, bf16[1,256,1024]{2,1,0:T(8,128)(2,1)S(1)} %copy-done, bf16[1,1024,256]{2,1,0:T(8,128)(2,1)S(1)} %copy-done.9, f32[384,256]{1,0:T(8,128)S(1)} %convolution_minimum_fusion), kind=kOutput, calls=%fused_computation.2 | convolution fusion | flops 403931136 | bytes 3014656 | tf_op jit(solution)/shard_map/dot_general | solution.py:134
  64.2 0.0 reduce-scatter.2.cloned.1.call-update
  64.3 21.3 %reduce-scatter.2.cloned.1.call-done = bf16[8,48,256]{2,1,0:T(8,128)(2,1)} async-done(((bf16[8,48,1024]{2,1,0:T(8,128)(2,1)}), bf16[8,48,256]{2,1,0:T(8,128)(2,1)}) %reduce-scatter.2.cloned.1.call-update) | async-done | bytes 196624 | tf_op jit(solution)/shard_map/reduce_scatter | solution.py:139
  85.6 5.5 %all-to-all-start.1 = ((bf16[8,48,256]{2,1,0:T(8,128)(2,1)}), bf16[8,48,256]{2,1,0:T(8,128)(2,1)S(1)}, u32[]{:S(2)}, u32[]{:S(2)}) async-start(bf16[8,48,256]{2,1,0:T(8,128)(2,1)} %reduce-scatter.2.cloned.1.call-done), calls=%async_computation.2 | async-start | bytes 393216 | tf_op jit(solution)/shard_map/all_to_all | solution.py:140
  91.1 0.1 mul.187
  91.2 0.1 copy.33
  91.3 7.6 %all-to-all-done.1 = bf16[8,48,256]{2,1,0:T(8,128)(2,1)S(1)} async-done(((bf16[8,48,256]{2,1,0:T(8,128)(2,1)}), bf16[8,48,256]{2,1,0:T(8,128)(2,1)S(1)}, u32[]{:S(2)}, u32[]{:S(2)}) %all-to-all-start.1) | async-done | bytes 196640 | tf_op jit(solution)/shard_map/all_to_all | solution.py:140
  98.9 1.0 gather_fusion
  99.9 0.2 multiply_reduce_fusion
  100.1 0.6 add_convert_fusion
  (34 shorter events, 0.3 us)
Async XLA Ops:
  7.2 55.2 %copy-start = (bf16[1,256,1024]{2,1,0:T(8,128)(2,1)S(1)}, bf16[1,256,1024]{2,1,0:T(8,128)(2,1)}, u32[]{:S(2)}) copy-start(bf16[1,256,1024]{2,1,0:T(8,128)(2,1)} %param.35) | copy-start | bytes 1572868
  7.2 78.4 %reduce-scatter.2.cloned.1.call-start = ((), (), s32[]{:S(2)}) async-start(), calls=%async_computation.3 | async-start | bytes 983040 | tf_op jit(solution)/shard_map/reduce_scatter | solution.py:139
  15.3 7.1 %copy-start.1 = (f32[48,2,64,64]{3,2,1,0:T(8,128)S(1)}, f32[48,2,64,64]{3,2,1,0:T(8,128)}, u32[]{:S(2)}) copy-start(f32[48,2,64,64]{3,2,1,0:T(8,128)} %param.19) | copy-start | bytes 4718596
  24.6 1.7 %copy-start.2 = (f32[48,2,64,64]{3,2,1,0:T(8,128)}, f32[48,2,64,64]{3,2,1,0:T(8,128)S(1)}, u32[]{:S(2)}) copy-start(f32[48,2,64,64]{3,2,1,0:T(8,128)S(1)} %multiply_add_fusion) | copy-start | bytes 4718596
  26.2 3.2 %copy-start.5 = (bf16[128,1024]{1,0:T(8,128)(2,1)S(1)}, bf16[128,1024]{1,0:T(8,128)(2,1)}, u32[]{:S(2)}) copy-start(bf16[128,1024]{1,0:T(8,128)(2,1)} %param.30) | copy-start | bytes 786436
  26.2 3.2 %copy-start.8 = (f32[128]{0:T(128)S(1)}, f32[128]{0:T(128)}, u32[]{:S(2)}) copy-start(f32[128]{0:T(128)} %param.29) | copy-start | bytes 1540
  26.2 11.4 %copy-start.3 = (bf16[48,1024]{1,0:T(8,128)(2,1)S(1)}, bf16[48,1024]{1,0:T(8,128)(2,1)}, u32[]{:S(2)}) copy-start(bf16[48,1024]{1,0:T(8,128)(2,1)} %param.18) | copy-start | bytes 294916
  26.2 11.6 %copy-start.6 = (s32[48,4]{0,1:T(4,128)S(1)}, s32[48,4]{0,1:T(4,128)}, u32[]{:S(2)}) copy-start(s32[48,4]{0,1:T(4,128)} %param.31) | copy-start | bytes 2308
  26.2 35.7 %copy-start.4 = (bf16[1,1024,256]{2,1,0:T(8,128)(2,1)S(1)}, bf16[1,1024,256]{2,1,0:T(8,128)(2,1)}, u32[]{:S(2)}) copy-start(bf16[1,1024,256]{2,1,0:T(8,128)(2,1)} %param.33) | copy-start | bytes 1572868
  28.8 33.6 %copy-start.9 = (bf16[1,1024,256]{2,1,0:T(8,128)(2,1)S(1)}, bf16[1,1024,256]{2,1,0:T(8,128)(2,1)}, u32[]{:S(2)}) copy-start(bf16[1,1024,256]{2,1,0:T(8,128)(2,1)} %param.34) | copy-start | bytes 1572868
  62.4 28.8 %copy-start.7 = (f32[48,4]{0,1:T(4,128)S(1)}, f32[48,4]{0,1:T(4,128)}, u32[]{:S(2)}) copy-start(f32[48,4]{0,1:T(4,128)} %param.32) | copy-start | bytes 2308
  85.6 13.3 %all-to-all-start.1 = ((bf16[8,48,256]{2,1,0:T(8,128)(2,1)}), bf16[8,48,256]{2,1,0:T(8,128)(2,1)S(1)}, u32[]{:S(2)}, u32[]{:S(2)}) async-start(bf16[8,48,256]{2,1,0:T(8,128)(2,1)} %reduce-scatter.2.cloned.1.call-done), calls=%async_computation.2 | async-start | bytes 393216 | tf_op jit(solution)/shard_map/all_to_all | solution.py:140
Sparse Core Ops, SparseCore 0:
  64.4 21.1 reduce-scatter.1
